TPU v7x, 32 devices: a whole 2x2x4 slice. The times are simulated.
32 devices in a mesh: ep: 4 (over y, x), tp: 8 (over z, core).
Axes of the slice: x: 2, y: 2, z: 4, core: 2. Of those that a mesh axis runs over, the one named last changes fastest.
Arguments:
- tokens: bfloat16 [128, 2048], P(('ep', 'tp')), may hold values from -6 to 6
- lengths: int32 [128], P(('ep', 'tp')), may hold values from 64 to 1024
- cache_latent: bfloat16 [128, 1024, 512], P(('ep', 'tp')), may hold values from -6 to 6
- cache_rope_key: bfloat16 [128, 1024, 32], P(('ep', 'tp')), may hold values from -1000 to 1000
- route_ids: int32 [128, 4], P('ep'), may hold values from 0 to 31, all different within a row; in each aligned block of 32 rows (0 to 31, 32 to 63, ...) at most 8 rows name the same one
- route_weights: float32 [128, 4], P('ep'), may hold values from 0.2 to 2
- attn_gain: float32 [2048], replicated, may hold values from 0.1 to 1.9
- w_query_nope: bfloat16 [2048, 16, 64], P(None, 'tp'), may hold values from -0.125 to 0.125
- w_query_rope: bfloat16 [2048, 16, 32], P(None, 'tp'), may hold values from -0.125 to 0.125
- w_latent_down: bfloat16 [2048, 512], P(None, 'tp'), may hold values from -0.125 to 0.125
- w_key_rope: bfloat16 [2048, 32], replicated, may hold values from -0.125 to 0.125
- latent_gain: float32 [512], replicated, may hold values from 0.1 to 1.9
- w_key_up: bfloat16 [512, 16, 64], P(None, 'tp'), may hold values from -0.75 to 0.75
- w_value_up: bfloat16 [512, 16, 64], P(None, 'tp'), may hold values from -0.25 to 0.25
- w_attn_out: bfloat16 [16, 64, 2048], P('tp'), may hold values from -0.1875 to 0.1875
- ffn_gain: float32 [2048], replicated, may hold values from 0.1 to 1.9
- expert_gate: bfloat16 [32, 2048, 512], P(('ep', 'tp')), may hold values from -0.125 to 0.125
- expert_up: bfloat16 [32, 2048, 512], P(('ep', 'tp')), may hold values from -0.125 to 0.125
- expert_down: bfloat16 [32, 512, 2048], P(('ep', 'tp')), may hold values from -0.25 to 0.25
- shared_gate: bfloat16 [2048, 512], P(None, 'tp'), may hold values from -0.125 to 0.125
- shared_up: bfloat16 [2048, 512], P(None, 'tp'), may hold values from -0.125 to 0.125
- shared_down: bfloat16 [512, 2048], P('tp'), may hold values from -0.25 to 0.25
- dense_gate: bfloat16 [2048, 1024], P(None, 'tp'), may hold values from -0.125 to 0.125
- dense_up: bfloat16 [2048, 1024], P(None, 'tp'), may hold values from -0.125 to 0.125
- dense_down: bfloat16 [1024, 2048], P('tp'), may hold values from -0.1875 to 0.1875
- branch_gate: bfloat16 [2048], replicated, may hold values from -0.125 to 0.125
Outputs:
- mixed: bfloat16 [128, 2048], P(('ep', 'tp'))
- new_latent: bfloat16 [128, 512], P(('ep', 'tp'))
- new_rope_key: bfloat16 [128, 32], P(('ep', 'tp'))
Inputs may be any that keep to these rules, and one draw needn't show every extreme that they name: `route_ids`: in each aligned block of 32 rows, no expert is named by more than 8 of the block's rows, a bound that some block reaches. Each row names 4 different experts.
All inputs are finite; a program needn't handle non-finite values.
Results may differ from a plain program's by a relative error of at most 0.025.
Values may be sent and summed in bfloat16 or wider, within the bound.
A program may use at most 64 MiB of HBM per device.

v0:
```python
import jax
import jax.numpy as jnp
from jax import lax
from jax.sharding import PartitionSpec as P

epsilon = 1e-06
rope_base = 10000.0


def norm_rows(values, scales):
    values = values.astype(jnp.float32)
    factor = lax.rsqrt(jnp.mean(values * values, axis=-1, keepdims=True) + epsilon)
    return values * factor * scales


def rotate(values, positions):
    half_dim = values.shape[-1] // 2
    frequencies = rope_base ** (-jnp.arange(half_dim).astype(jnp.float32) / half_dim)
    angles = positions.astype(jnp.float32)[:, None] * frequencies[None, :]
    bcast_shape = (angles.shape[0],) + (1,) * (values.ndim - 2) + (half_dim,)
    cosine = jnp.cos(angles).reshape(bcast_shape)
    sine_val = jnp.sin(angles).reshape(bcast_shape)
    first_half = values[..., :half_dim].astype(jnp.float32)
    second_half = values[..., half_dim:].astype(jnp.float32)
    return jnp.concatenate(
        [
            first_half * cosine - second_half * sine_val,
            first_half * sine_val + second_half * cosine,
        ],
        axis=-1,
    )


def swiglu(inputs, gate_w, up_w):
    gate_val = jnp.dot(inputs, gate_w, preferred_element_type=jnp.float32)
    up_val = jnp.dot(inputs, up_w, preferred_element_type=jnp.float32)
    return (jax.nn.silu(gate_val) * up_val).astype(jnp.bfloat16)


def local(
    tokens,
    lengths,
    cache_latent,
    cache_rope_key,
    route_ids,
    route_weights,
    attn_gain,
    w_query_nope,
    w_query_rope,
    w_latent_down,
    w_key_rope,
    latent_gain,
    w_key_up,
    w_value_up,
    w_attn_out,
    ffn_gain,
    expert_gate,
    expert_up,
    expert_down,
    shared_gate,
    shared_up,
    shared_down,
    dense_gate,
    dense_up,
    dense_down,
    branch_gate,
):
    own_rows, model_width = tokens.shape
    tp_count = lax.axis_size("tp")
    ep_count = lax.axis_size("ep")
    tp_index = lax.axis_index("tp")
    local_heads = w_query_nope.shape[1]
    head_scale = (w_query_nope.shape[2] + w_query_rope.shape[2]) ** (-0.5)
    normed = norm_rows(tokens, attn_gain).astype(jnp.bfloat16)
    group_in = lax.all_gather(normed, "tp", axis=0, tiled=True)
    group_rows = group_in.shape[0]
    query_nope = jnp.dot(
        group_in, w_query_nope.reshape(model_width, -1), preferred_element_type=jnp.float32
    )
    query_nope = query_nope.astype(jnp.bfloat16).reshape(group_rows, local_heads, -1)
    query_latent = jnp.einsum(
        "ghn,rhn->ghr", query_nope, w_key_up, preferred_element_type=jnp.float32
    ).astype(jnp.bfloat16)
    query_rope = jnp.dot(
        group_in, w_query_rope.reshape(model_width, -1), preferred_element_type=jnp.float32
    )
    query_rope = query_rope.astype(jnp.bfloat16).reshape(group_rows, local_heads, -1)
    latent_part = jnp.dot(group_in, w_latent_down, preferred_element_type=jnp.float32).astype(
        jnp.bfloat16
    )
    own_latent_q, own_rope_q, latent_raw = (
        lax.all_to_all(query_latent, "tp", split_axis=0, concat_axis=1, tiled=True),
        lax.all_to_all(query_rope, "tp", split_axis=0, concat_axis=1, tiled=True),
        lax.all_to_all(latent_part, "tp", split_axis=0, concat_axis=1, tiled=True),
    )
    new_latent = norm_rows(latent_raw, latent_gain).astype(jnp.bfloat16)
    key_rope = jnp.dot(normed, w_key_rope, preferred_element_type=jnp.float32)
    new_rope = rotate(key_rope, lengths).astype(jnp.bfloat16)
    query_rot = rotate(own_rope_q, lengths).astype(jnp.bfloat16)
    scores = jnp.einsum(
        "bhr,blr->bhl", own_latent_q, cache_latent, preferred_element_type=jnp.float32
    )
    scores = scores + jnp.einsum(
        "bhe,ble->bhl", query_rot, cache_rope_key, preferred_element_type=jnp.float32
    )
    scores = scores * head_scale
    in_range = (
        jnp.arange(cache_latent.shape[1], dtype=jnp.int32)[None, None, :] < lengths[:, None, None]
    )
    scores = jnp.where(in_range, scores, -jnp.inf)
    own_score = jnp.einsum(
        "bhr,br->bh", own_latent_q, new_latent, preferred_element_type=jnp.float32
    )
    own_score = (
        own_score
        + jnp.einsum("bhe,be->bh", query_rot, new_rope, preferred_element_type=jnp.float32)
    ) * head_scale
    peak_score = jnp.maximum(jnp.max(scores, axis=-1), own_score)
    past_exp = jnp.exp(scores - peak_score[..., None])
    own_exp = jnp.exp(own_score - peak_score)
    total_exp = jnp.sum(past_exp, axis=-1) + own_exp
    past_weight = (past_exp / total_exp[..., None]).astype(jnp.bfloat16)
    own_weight = (own_exp / total_exp).astype(jnp.bfloat16)
    out_latent = jnp.einsum(
        "bhl,blr->bhr", past_weight, cache_latent, preferred_element_type=jnp.float32
    )
    out_latent = (
        out_latent
        + own_weight.astype(jnp.float32)[..., None] * new_latent.astype(jnp.float32)[:, None, :]
    )
    out_latent = out_latent.astype(jnp.bfloat16)
    head_latent = lax.all_to_all(out_latent, "tp", split_axis=1, concat_axis=0, tiled=True)
    head_values = jnp.einsum(
        "ghr,rhv->ghv", head_latent, w_value_up, preferred_element_type=jnp.float32
    ).astype(jnp.bfloat16)
    attn_part = jnp.dot(
        head_values.reshape(group_rows, -1),
        w_attn_out.reshape(-1, model_width),
        preferred_element_type=jnp.float32,
    )
    own_start = tp_index * own_rows
    placed = lax.dynamic_update_slice_in_dim(
        jnp.zeros((group_rows, model_width), jnp.float32), tokens.astype(jnp.float32), own_start, 0
    )
    group_after = lax.psum((attn_part + placed).astype(jnp.bfloat16), "tp").astype(jnp.float32)
    ffn_in = norm_rows(group_after, ffn_gain).astype(jnp.bfloat16)
    after_attn = lax.dynamic_slice_in_dim(group_after, own_start, own_rows, 0)
    shared_term = jnp.dot(
        swiglu(ffn_in, shared_gate, shared_up), shared_down, preferred_element_type=jnp.float32
    )
    branch_mix = jax.nn.sigmoid(jnp.dot(ffn_in, branch_gate, preferred_element_type=jnp.float32))
    dense_term = branch_mix[:, None] * jnp.dot(
        swiglu(ffn_in, dense_gate, dense_up), dense_down, preferred_element_type=jnp.float32
    )
    top_count = route_ids.shape[1]
    expert_local = expert_gate.shape[0]
    capacity = max(
        2, (2 * own_rows * top_count + expert_local * ep_count - 1) // (expert_local * ep_count)
    )
    target_count = ep_count * expert_local
    slot_count = target_count * capacity
    column = route_ids // expert_local % tp_count
    target = route_ids // (expert_local * tp_count) * expert_local + route_ids % expert_local
    flat_target = jnp.where(column == tp_index, target, -1).reshape(-1)
    target_hits = (
        flat_target[:, None] == jnp.arange(target_count, dtype=jnp.int32)[None, :]
    ).astype(jnp.int32)
    earlier = jnp.cumsum(target_hits, axis=0) - target_hits
    rank_in = jnp.sum(earlier * target_hits, axis=1)
    slot_index = jnp.where(flat_target >= 0, flat_target * capacity + rank_in, -1).reshape(
        group_rows, top_count
    )
    slot_match = slot_index[:, :, None] == jnp.arange(slot_count, dtype=jnp.int32)[None, None, :]
    dispatch = jnp.any(slot_match, axis=1).astype(jnp.bfloat16)
    combine = jnp.sum(jnp.where(slot_match, route_weights[:, :, None], 0.0), axis=1)
    outgoing = jnp.einsum("gs,gd->sd", dispatch, ffn_in, preferred_element_type=jnp.float32).astype(
        jnp.bfloat16
    )
    outgoing = outgoing.reshape(ep_count, expert_local, capacity, model_width)
    arrived = lax.all_to_all(outgoing, "ep", split_axis=0, concat_axis=0, tiled=True)
    gate_val = jnp.einsum(
        "sxcd,xdf->sxcf", arrived, expert_gate, preferred_element_type=jnp.float32
    )
    up_val = jnp.einsum("sxcd,xdf->sxcf", arrived, expert_up, preferred_element_type=jnp.float32)
    act_val = (jax.nn.silu(gate_val) * up_val).astype(jnp.bfloat16)
    result = jnp.einsum(
        "sxcf,xfd->sxcd", act_val, expert_down, preferred_element_type=jnp.float32
    ).astype(jnp.bfloat16)
    returned = lax.all_to_all(result, "ep", split_axis=0, concat_axis=0, tiled=True)
    routed = jnp.dot(
        combine,
        returned.reshape(slot_count, model_width).astype(jnp.float32),
        precision=lax.Precision.HIGHEST,
    )
    ffn_total = routed + shared_term + dense_term
    mixed = (
        after_attn
        + lax.psum_scatter(
            ffn_total.astype(jnp.bfloat16), "tp", scatter_dimension=0, tiled=True
        ).astype(jnp.float32)
    ).astype(jnp.bfloat16)
    return (mixed, new_latent, new_rope)


def solution(mesh):
    in_specs = (
        P(("ep", "tp"), None),
        P(("ep", "tp")),
        P(("ep", "tp"), None, None),
        P(("ep", "tp"), None, None),
        P("ep", None),
        P("ep", None),
        P(),
        P(None, "tp", None),
        P(None, "tp", None),
        P(None, "tp"),
        P(),
        P(),
        P(None, "tp", None),
        P(None, "tp", None),
        P("tp", None, None),
        P(),
        P(("ep", "tp"), None, None),
        P(("ep", "tp"), None, None),
        P(("ep", "tp"), None, None),
        P(None, "tp"),
        P(None, "tp"),
        P("tp", None),
        P(None, "tp"),
        P(None, "tp"),
        P("tp", None),
        P(),
    )
    out_specs = (P(("ep", "tp"), None), P(("ep", "tp"), None), P(("ep", "tp"), None))
    return jax.shard_map(local, mesh=mesh, in_specs=in_specs, out_specs=out_specs, check_vma=False)
```

profile of v0, /device:TPU:0, one launch (start us, length us, event | category | flops | bytes accessed | tf_op | source)
XLA Modules:
  0.0 222.2 jit_solution(12282794214563576408)
XLA Ops:
  7.2 1.0 fusion.58
  8.2 0.8 fusion.95
  9.1 15.7 %all-gather = bf16[8,4,2048]{2,1,0:T(4,128)(2,1)S(1)} all-gather(bf16[1,4,2048]{2,1,0:T(4,128)(2,1)S(1)} %fusion.95), channel_id=1, replica_groups=mesh['ep'=4,'tp'=8] {'tp'}, dimensions={0}, use_global_device_ids=true | all-gather | bytes 147456 | tf_op jit(solution)/shard_map/all_gather | solution.py:75
  24.8 1.1 convolution_convert_fusion.5
  26.0 0.7 reshape.224
  26.7 4.6 %all-to-all-start.2 = ((bf16[8,2,128]{2,1,0:T(2,128)(2,1)}), bf16[8,2,128]{2,1,0:T(2,128)(2,1)S(1)}, u32[]{:S(2)}, u32[]{:S(2)}) async-start(bf16[8,2,128]{2,1,0:T(2,128)(2,1)} %reshape.224), calls=%async_computation.2 | async-start | bytes 8192 | tf_op jit(solution)/shard_map/all_to_all | solution.py:94
  31.3 0.7 convert_element_type.145
  31.9 0.7 iota_compare_fusion.2
  32.7 1.1 fusion.93
  33.8 0.8 copy.71
  34.6 0.1 eq.39
  34.7 0.1 fusion.53
  34.8 0.2 reduce_window_sum.11
  35.0 0.2 select_reduce_fusion.1
  35.1 0.1 reduce_sum.60
  35.3 1.1 convolution_convert_fusion.6
  36.4 1.3 convolution_convert_fusion.4
  37.8 0.1 reshape.198
  37.9 0.1 fusion.12
  38.0 0.1 subtract_convert_fusion
  38.2 0.6 reshape.219
  38.9 0.1 reshape.200
  39.0 0.7 reshape.222
  39.7 0.7 copy.64
  40.4 0.6 dynamic-slice.1
  41.6 5.1 %all-to-all-start.1 = ((bf16[8,2,128]{2,1,0:T(2,128)(2,1)}), bf16[8,2,128]{2,1,0:T(2,128)(2,1)S(1)}, u32[]{:S(2)}, u32[]{:S(2)}) async-start(bf16[8,2,128]{2,1,0:T(2,128)(2,1)} %reshape.222), calls=%async_computation.1 | async-start | bytes 8192 | tf_op jit(solution)/shard_map/all_to_all | solution.py:93
  46.7 0.1 reshape.225
  46.8 0.1 fusion.63
  47.0 5.2 %all-to-all-done.1 = bf16[8,2,128]{2,1,0:T(2,128)(2,1)S(1)} async-done(((bf16[8,2,128]{2,1,0:T(2,128)(2,1)}), bf16[8,2,128]{2,1,0:T(2,128)(2,1)S(1)}, u32[]{:S(2)}, u32[]{:S(2)}) %all-to-all-start.1) | async-done | bytes 4128 | tf_op jit(solution)/shard_map/all_to_all | solution.py:93
  52.2 3.3 %all-to-all-start = ((bf16[32,2,512]{2,1,0:T(2,128)(2,1)}), bf16[32,2,512]{2,1,0:T(2,128)(2,1)S(1)}, u32[]{:S(2)}, u32[]{:S(2)}) async-start(bf16[32,2,512]{2,1,0:T(2,128)(2,1)} %copy.64), calls=%async_computation | async-start | bytes 131072 | tf_op jit(solution)/shard_map/all_to_all | solution.py:92
  55.6 0.1 reshape.223
  55.8 0.1 fusion.55
  55.9 0.2 fusion.83
  56.0 5.4 %all-to-all-done = bf16[32,2,512]{2,1,0:T(2,128)(2,1)S(1)} async-done(((bf16[32,2,512]{2,1,0:T(2,128)(2,1)}), bf16[32,2,512]{2,1,0:T(2,128)(2,1)S(1)}, u32[]{:S(2)}, u32[]{:S(2)}) %all-to-all-start) | async-done | bytes 65568 | tf_op jit(solution)/shard_map/all_to_all | solution.py:92
  61.5 0.1 fusion.79
  61.7 3.5 %fusion.100 = f32[4,16,1024]{2,1,0:T(8,128)S(1)} fusion(bf16[4,16,512]{2,1,0:T(8,128)(2,1)S(1)} %all_to_all.58, bf16[4,1024,512]{2,1,0:T(8,128)(2,1)} %param.28), kind=kOutput, calls=%fused_computation.141 | convolution fusion | flops 67108864 | bytes 4521984 | tf_op jit(solution)/shard_map/bhr,blr->bhl/dot_general | solution.py:100
  65.2 0.3 fusion.99
  65.5 0.2 fusion.37
  65.8 0.7 fusion.11
  66.5 0.7 copy.68
  67.2 3.3 %all-to-all-start.3 = ((bf16[4,16,512]{2,0,1:T(4,128)(2,1)}), bf16[4,16,512]{2,0,1:T(4,128)(2,1)S(1)}, u32[]{:S(2)}, u32[]{:S(2)}) async-start(bf16[4,16,512]{2,0,1:T(4,128)(2,1)} %copy.68), calls=%async_computation.3 | async-start | bytes 131072 | tf_op jit(solution)/shard_map/all_to_all | solution.py:132
  70.6 0.7 select_reduce_fusion
  71.3 5.1 %all-to-all-done.3 = bf16[4,16,512]{2,0,1:T(4,128)(2,1)S(1)} async-done(((bf16[4,16,512]{2,0,1:T(4,128)(2,1)}), bf16[4,16,512]{2,0,1:T(4,128)(2,1)S(1)}, u32[]{:S(2)}, u32[]{:S(2)}) %all-to-all-start.3) | async-done | bytes 65568 | tf_op jit(solution)/shard_map/all_to_all | solution.py:132
  76.5 1.3 convolution_bitcast_fusion
  77.8 0.7 convert_element_type.161
  78.5 0.1 fusion.52
  78.6 53.5 %all-reduce.4.cloned.1.call-done = bf16[32,2048]{1,0:T(8,128)(2,1)} async-done(((bf16[32,2048]{1,0:T(8,128)(2,1)}), bf16[32,2048]{1,0:T(8,128)(2,1)}) %all-reduce.4.cloned.1.call-update) | async-done | bytes 131088 | tf_op jit(solution)/shard_map/psum | solution.py:145
  132.1 1.0 multiply_reduce_fusion
  133.2 1.8 fusion.2
  135.0 3.6 %all-to-all-start.4 = ((bf16[4,1,8,2048]{3,2,1,0:T(8,128)(2,1)}), bf16[4,1,8,2048]{3,2,1,0:T(8,128)(2,1)S(1)}, u32[]{:S(2)}, u32[]{:S(2)}) async-start(bf16[4,1,8,2048]{3,2,1,0:T(8,128)(2,1)} %fusion.2), calls=%async_computation.4 | async-start | bytes 262144 | tf_op jit(solution)/shard_map/all_to_all | solution.py:180
  138.6 1.8 fusion.96
  140.4 1.9 fusion.97
  142.3 1.4 all-to-all-done.4
  143.7 2.0 fusion.13
  145.7 3.2 %fusion.3 = bf16[4,1,8,2048]{3,2,1,0:T(8,128)(2,1)} fusion(bf16[1,512,2048]{2,1,0:T(8,128)(2,1)S(1)} %copy-done, bf16[1,2048,512]{2,1,0:T(8,128)(2,1)} %param.43, bf16[4,1,8,2048]{3,2,1,0:T(8,128)(2,1)S(1)} %all-to-all-done.4, f32[4,1,8,512]{3,2,0,1:T(8,128)S(1)} %fusion.13), kind=kOutput, calls=%fused_computation.8 | convolution fusion | flops 134381568 | bytes 4521984 | tf_op jit(solution)/shard_map/sxcf,xfd->sxcd/dot_general | solution.py:186
  148.9 3.5 %all-to-all-start.5 = ((bf16[4,1,8,2048]{3,2,1,0:T(8,128)(2,1)}), bf16[4,1,8,2048]{3,2,1,0:T(8,128)(2,1)S(1)}, u32[]{:S(2)}, u32[]{:S(2)}) async-start(bf16[4,1,8,2048]{3,2,1,0:T(8,128)(2,1)} %fusion.3), calls=%async_computation.5 | async-start | bytes 262144 | tf_op jit(solution)/shard_map/all_to_all | solution.py:189
  152.5 0.7 fusion.34
  153.2 4.2 %all-to-all-done.5 = bf16[4,1,8,2048]{3,2,1,0:T(8,128)(2,1)S(1)} async-done(((bf16[4,1,8,2048]{3,2,1,0:T(8,128)(2,1)}), bf16[4,1,8,2048]{3,2,1,0:T(8,128)(2,1)S(1)}, u32[]{:S(2)}, u32[]{:S(2)}) %all-to-all-start.5) | async-done | bytes 131104 | tf_op jit(solution)/shard_map/all_to_all | solution.py:189
  157.4 0.2 fusion.38
  157.6 1.4 convolution_add_fusion
  159.1 2.2 fusion.1
  161.3 1.3 pad_maximum_fusion.3
  162.6 51.4 %all-reduce.6.cloned.1.call-done = bf16[32,2048]{1,0:T(8,128)(2,1)} async-done(((bf16[32,2048]{1,0:T(8,128)(2,1)}), bf16[32,2048]{1,0:T(8,128)(2,1)}) %all-reduce.6.cloned.1.call-update) | async-done | bytes 131088
  214.0 1.4 add_convert_fusion
  (64 shorter events, 0.9 us)
Async XLA Ops:
  7.2 138.5 %copy-start = (bf16[1,512,2048]{2,1,0:T(8,128)(2,1)S(1)}, bf16[1,512,2048]{2,1,0:T(8,128)(2,1)}, u32[]{:S(2)}) copy-start(bf16[1,512,2048]{2,1,0:T(8,128)(2,1)} %param.44) | copy-start | bytes 6291460
  7.2 33.2 %copy-start.18 = (u32[32]{0:T(128)S(1)}, u32[32]{0:T(128)}, u32[]{:S(2)}) copy-start(u32[32]{0:T(128)} %constant.109) | copy-start | bytes 388
  7.2 30.7 %copy-start.10 = (bf16[512,2,64]{0,2,1:T(8,128)(2,1)S(1)}, bf16[512,2,64]{0,2,1:T(8,128)(2,1)}, u32[]{:S(2)}) copy-start(bf16[512,2,64]{0,2,1:T(8,128)(2,1)} %param.38) | copy-start | bytes 393220
  7.2 31.0 %copy-start.14 = (bf16[2048]{0:T(1024)(128)(2,1)S(1)}, bf16[2048]{0:T(1024)(128)(2,1)}, u32[]{:S(2)}) copy-start(bf16[2048]{0:T(1024)(128)(2,1)} %param.51) | copy-start | bytes 12292
  7.2 48.5 %copy-start.16 = (f32[512]{0:T(512)S(1)}, f32[512]{0:T(512)}, u32[]{:S(2)}) copy-start(f32[512]{0:T(512)} %param.37) | copy-start | bytes 6148
  26.7 14.9 %all-to-all-start.2 = ((bf16[8,2,128]{2,1,0:T(2,128)(2,1)}), bf16[8,2,128]{2,1,0:T(2,128)(2,1)S(1)}, u32[]{:S(2)}, u32[]{:S(2)}) async-start(bf16[8,2,128]{2,1,0:T(2,128)(2,1)} %reshape.224), calls=%async_computation.2 | async-start | bytes 8192 | tf_op jit(solution)/shard_map/all_to_all | solution.py:94
  38.1 23.3 %copy-start.12 = (bf16[4,16]{1,0:T(4,128)(2,1)}, bf16[4,16]{1,0:T(4,128)(2,1)S(1)}, u32[]{:S(2)}) copy-start(bf16[4,16]{1,0:T(4,128)(2,1)S(1)} %get-tuple-element.10) | copy-start | bytes 388
  41.6 10.6 %all-to-all-start.1 = ((bf16[8,2,128]{2,1,0:T(2,128)(2,1)}), bf16[8,2,128]{2,1,0:T(2,128)(2,1)S(1)}, u32[]{:S(2)}, u32[]{:S(2)}) async-start(bf16[8,2,128]{2,1,0:T(2,128)(2,1)} %reshape.222), calls=%async_computation.1 | async-start | bytes 8192 | tf_op jit(solution)/shard_map/all_to_all | solution.py:93
  52.2 9.2 %all-to-all-start = ((bf16[32,2,512]{2,1,0:T(2,128)(2,1)}), bf16[32,2,512]{2,1,0:T(2,128)(2,1)S(1)}, u32[]{:S(2)}, u32[]{:S(2)}) async-start(bf16[32,2,512]{2,1,0:T(2,128)(2,1)} %copy.64), calls=%async_computation | async-start | bytes 131072 | tf_op jit(solution)/shard_map/all_to_all | solution.py:92
  55.8 9.4 %copy-start.15 = (bf16[4,512]{1,0:T(4,128)(2,1)}, bf16[4,512]{1,0:T(4,128)(2,1)S(1)}, u32[]{:S(2)}) copy-start(bf16[4,512]{1,0:T(4,128)(2,1)S(1)} %get-tuple-element.4) | copy-start | bytes 12292
  61.6 3.5 %copy-start.6 = (bf16[4,1024,32]{1,2,0:T(8,128)(2,1)S(1)}, bf16[4,1024,32]{1,2,0:T(8,128)(2,1)}, u32[]{:S(2)}) copy-start(bf16[4,1024,32]{1,2,0:T(8,128)(2,1)} %param.29) | copy-start | bytes 786436
  61.6 4.1 %copy-start.1 = (bf16[4,1024,512]{2,1,0:T(8,128)(2,1)S(1)}, bf16[4,1024,512]{2,1,0:T(8,128)(2,1)}, u32[]{:S(2)}) copy-start(bf16[4,1024,512]{2,1,0:T(8,128)(2,1)} %param.28) | copy-start | bytes 12582916
  65.8 4.8 %copy-start.17 = (f32[32,4]{0,1:T(4,128)S(1)}, f32[32,4]{0,1:T(4,128)}, u32[]{:S(2)}) copy-start(f32[32,4]{0,1:T(4,128)} %param.31) | copy-start | bytes 1540
  65.8 10.7 %copy-start.4 = (bf16[2,64,2048]{2,1,0:T(8,128)(2,1)S(1)}, bf16[2,64,2048]{2,1,0:T(8,128)(2,1)}, u32[]{:S(2)}) copy-start(bf16[2,64,2048]{2,1,0:T(8,128)(2,1)} %param.40) | copy-start | bytes 1572868
  65.8 12.0 %copy-start.9 = (bf16[4,2048]{1,0:T(4,128)(2,1)S(1)}, bf16[4,2048]{1,0:T(4,128)(2,1)}, u32[]{:S(2)}) copy-start(bf16[4,2048]{1,0:T(4,128)(2,1)} %param.26) | copy-start | bytes 49156
  66.5 66.7 %copy-start.8 = (f32[2048]{0:T(1024)S(1)}, f32[2048]{0:T(1024)}, u32[]{:S(2)}) copy-start(f32[2048]{0:T(1024)} %param.41) | copy-start | bytes 24580
  66.5 72.1 %copy-start.3 = (bf16[2048,128]{1,0:T(8,128)(2,1)S(1)}, bf16[2048,128]{1,0:T(8,128)(2,1)}, u32[]{:S(2)}) copy-start(bf16[2048,128]{1,0:T(8,128)(2,1)} %param.48) | copy-start | bytes 1572868
  67.2 9.2 %all-to-all-start.3 = ((bf16[4,16,512]{2,0,1:T(4,128)(2,1)}), bf16[4,16,512]{2,0,1:T(4,128)(2,1)S(1)}, u32[]{:S(2)}, u32[]{:S(2)}) async-start(bf16[4,16,512]{2,0,1:T(4,128)(2,1)} %copy.68), calls=%async_computation.3 | async-start | bytes 131072 | tf_op jit(solution)/shard_map/all_to_all | solution.py:132
  70.5 61.6 %all-reduce.4.cloned.1.call-start = ((), (), s32[]{:S(2)}) async-start(), calls=%async_computation.6 | async-start | bytes 262144 | tf_op jit(solution)/shard_map/psum | solution.py:145
  135.0 8.7 %all-to-all-start.4 = ((bf16[4,1,8,2048]{3,2,1,0:T(8,128)(2,1)}), bf16[4,1,8,2048]{3,2,1,0:T(8,128)(2,1)S(1)}, u32[]{:S(2)}, u32[]{:S(2)}) async-start(bf16[4,1,8,2048]{3,2,1,0:T(8,128)(2,1)} %fusion.2), calls=%async_computation.4 | async-start | bytes 262144 | tf_op jit(solution)/shard_map/all_to_all | solution.py:180
  145.7 6.7 %copy-start.2 = (bf16[32,2048]{1,0:T(8,128)(2,1)S(1)}, bf16[32,2048]{1,0:T(8,128)(2,1)}, u32[]{:S(2)}) copy-start(bf16[32,2048]{1,0:T(8,128)(2,1)} %all-reduce.4.cloned.1.call-done) | copy-start | bytes 393220
  145.7 6.7 %copy-start.13 = (bf16[2048,1]{0,1:T(2,128)(2,1)S(1)}, bf16[2048,1]{0,1:T(2,128)(2,1)}, u32[]{:S(2)}) copy-start(bf16[2048,1]{0,1:T(2,128)(2,1)} %reshape.219) | copy-start | bytes 12292
  145.7 11.7 %copy-start.11 = (f32[32,32]{1,0:T(8,128)S(1)}, f32[32,32]{1,0:T(8,128)}, u32[]{:S(2)}) copy-start(f32[32,32]{1,0:T(8,128)} %select_reduce_fusion) | copy-start | bytes 12292
  145.7 11.9 %copy-start.7 = (bf16[64,2048]{1,0:T(8,128)(2,1)S(1)}, bf16[64,2048]{1,0:T(8,128)(2,1)}, u32[]{:S(2)}) copy-start(bf16[64,2048]{1,0:T(8,128)(2,1)} %param.47) | copy-start | bytes 786436
  148.9 10.2 %copy-start.5 = (bf16[128,2048]{1,0:T(8,128)(2,1)S(1)}, bf16[128,2048]{1,0:T(8,128)(2,1)}, u32[]{:S(2)}) copy-start(bf16[128,2048]{1,0:T(8,128)(2,1)} %param.50) | copy-start | bytes 1572868
  148.9 8.4 %all-to-all-start.5 = ((bf16[4,1,8,2048]{3,2,1,0:T(8,128)(2,1)}), bf16[4,1,8,2048]{3,2,1,0:T(8,128)(2,1)S(1)}, u32[]{:S(2)}, u32[]{:S(2)}) async-start(bf16[4,1,8,2048]{3,2,1,0:T(8,128)(2,1)} %fusion.3), calls=%async_computation.5 | async-start | bytes 262144 | tf_op jit(solution)/shard_map/all_to_all | solution.py:189
  152.4 61.6 %all-reduce.6.cloned.1.call-start = ((), (), s32[]{:S(2)}) async-start(), calls=%async_computation.7 | async-start | bytes 262144
Sparse Core Ops, SparseCore 0:
  78.6 53.4 all-reduce.3
  161.4 52.5 all-reduce.5
where the time goes:
time: 223 us; the launch traced here: 222 us
  waiting for transfers between devices  126 us (57%)
  matrix products  26.3 us (12%)
  starting transfers between devices  23.6 us (11%)
  blocking collectives  15.7 us (7%)
  between operations  15.1 us (7%)
  other arithmetic  9.66 us (4%)
  local copies, waits for them, and re-layouts  5.69 us (3%)
    psum x1, waiting for transfers between devices, local(): lax.psum((attn_part + placed).astype(jnp.bfloat16), 'tp')  53.5 us
    unnamed x3, waiting for transfers between devices  51.4 us
    all_gather x1, blocking collectives, local(): group_in = lax.all_gather(normed, 'tp', axis=0, tiled=True)  15.7 us
    all_to_all x1, waiting for transfers between devices, local(): lax.all_to_all(query_latent, 'tp', split_axis=0, concat_axis=1, tiled=True)  5.38 us
    all_to_all x1, waiting for transfers between devices, local(): lax.all_to_all(query_rope, 'tp', split_axis=0, concat_axis=1, tiled=True)  5.2 us
    all_to_all x1, starting transfers between devices, local(): lax.all_to_all(query_rope, 'tp', split_axis=0, concat_axis=1, tiled=True)  5.11 us
    all_to_all x1, waiting for transfers between devices, local(): lax.all_to_all(out_latent, 'tp', split_axis=1, concat_axis=0, tiled=True)  5.08 us
    all_to_all x1, starting transfers between devices, local(): lax.all_to_all(latent_part, 'tp', split_axis=0, concat_axis=1, tiled=True)  4.6 us
  transfers between devices with their start and end apart: 8, of which 7 were waited for; matrix products, arithmetic and copies ran while one was open for 8% of the time, Pallas kernels for 0%

commit v1 on v0

--- a/solution.py
+++ b/solution.py
@@ -142,7 +142,9 @@
     placed = lax.dynamic_update_slice_in_dim(
         jnp.zeros((group_rows, model_width), jnp.float32), tokens.astype(jnp.float32), own_start, 0
     )
-    group_after = lax.psum((attn_part + placed).astype(jnp.bfloat16), "tp").astype(jnp.float32)
+    group_after = jnp.sum(
+        lax.all_gather((attn_part + placed).astype(jnp.bfloat16), "tp"), axis=0
+    ).astype(jnp.float32)
     ffn_in = norm_rows(group_after, ffn_gain).astype(jnp.bfloat16)
     after_attn = lax.dynamic_slice_in_dim(group_after, own_start, own_rows, 0)
     shared_term = jnp.dot(

time: 223 us -> 188 us (0.84)
  waiting for transfers between devices: 126 us -> 97 us
  matrix products: 26.3 us -> 21.8 us
    psum x1 -> x0, waiting for transfers between devices: 53.5 us -> none  [local(): lax.psum((attn_part + placed).astype(jnp.bfloat16), 'tp')]
    all_gather x0 -> x1, waiting for transfers between devices: none -> 18.5 us  [local(): lax.all_gather((attn_part + placed).astype(jnp.bfloat16), 'tp')]
    all_to_all x1, waiting for transfers between devices: 1.36 us -> 4.76 us  [local(): lax.all_to_all(outgoing, 'ep', split_axis=0, concat_axis=0, tiled=True)]
    dot_general x2, matrix products: 3.66 us -> 0.51 us  [swiglu(): gate_val = jnp.dot(inputs, gate_w, preferred_element_type=jnp.float32)]
  transfers between devices with their start and end apart: 8 -> 8, of which waited for: 7 -> 7; matrix products, arithmetic and copies ran while one was open for 8% -> 6% of each run, Pallas kernels for 0% -> 0%
where the time goes in v1:
time: 188 us; the launch traced here: 186 us
  waiting for transfers between devices  97 us (52%)
  starting transfers between devices  23.6 us (13%)
  matrix products  21.8 us (12%)
  blocking collectives  15.7 us (8%)
  between operations  15.1 us (8%)
  other arithmetic  8.86 us (5%)
  local copies, waits for them, and re-layouts  4.43 us (2%)
    unnamed x3, waiting for transfers between devices  52.7 us
    all_gather x1, waiting for transfers between devices, local(): lax.all_gather((attn_part + placed).astype(jnp.bfloat16), 'tp')  18.5 us
    all_gather x1, blocking collectives, local(): group_in = lax.all_gather(normed, 'tp', axis=0, tiled=True)  15.7 us
    all_to_all x1, waiting for transfers between devices, local(): lax.all_to_all(out_latent, 'tp', split_axis=1, concat_axis=0, tiled=True)  5.79 us
    all_to_all x1, waiting for transfers between devices, local(): lax.all_to_all(query_rope, 'tp', split_axis=0, concat_axis=1, tiled=True)  5.3 us
    all_to_all x1, waiting for transfers between devices, local(): lax.all_to_all(query_latent, 'tp', split_axis=0, concat_axis=1, tiled=True)  5.28 us
    all_to_all x1, starting transfers between devices, local(): lax.all_to_all(query_rope, 'tp', split_axis=0, concat_axis=1, tiled=True)  5.1 us
    all_to_all x1, waiting for transfers between devices, local(): lax.all_to_all(outgoing, 'ep', split_axis=0, concat_axis=0, tiled=True)  4.76 us
  transfers between devices with their start and end apart: 8, of which 7 were waited for; matrix products, arithmetic and copies ran while one was open for 6% of the time, Pallas kernels for 0%

profile of v1, /device:TPU:0, one launch (start us, length us, event | category | flops | bytes accessed | tf_op | source)
XLA Modules:
  0.0 186.5 jit_solution(12822232866815691506)
XLA Ops:
  7.2 1.0 fusion.58
  8.2 0.8 fusion.95
  9.0 15.7 %all-gather.1 = bf16[8,4,2048]{2,1,0:T(4,128)(2,1)S(1)} all-gather(bf16[1,4,2048]{2,1,0:T(4,128)(2,1)S(1)} %fusion.95), channel_id=1, replica_groups=mesh['ep'=4,'tp'=8] {'tp'}, dimensions={0}, use_global_device_ids=true | all-gather | bytes 147456 | tf_op jit(solution)/shard_map/all_gather | solution.py:75
  24.8 1.1 convolution_convert_fusion.5
  25.9 0.7 reshape.225
  26.6 4.6 %all-to-all-start.2 = ((bf16[8,2,128]{2,1,0:T(2,128)(2,1)}), bf16[8,2,128]{2,1,0:T(2,128)(2,1)S(1)}, u32[]{:S(2)}, u32[]{:S(2)}) async-start(bf16[8,2,128]{2,1,0:T(2,128)(2,1)} %reshape.225), calls=%async_computation.2 | async-start | bytes 8192 | tf_op jit(solution)/shard_map/all_to_all | solution.py:94
  31.2 0.7 convert_element_type.147
  31.9 0.7 iota_compare_fusion.2
  32.6 1.1 fusion.93
  33.8 1.1 convolution_convert_fusion.6
  34.9 1.3 convolution_convert_fusion.4
  36.2 0.1 reshape.198
  36.4 0.1 fusion.12
  36.5 0.1 subtract_convert_fusion
  36.7 0.1 reshape.200
  36.8 0.7 reshape.223
  37.5 0.7 copy.64
  38.2 5.1 %all-to-all-start.1 = ((bf16[8,2,128]{2,1,0:T(2,128)(2,1)}), bf16[8,2,128]{2,1,0:T(2,128)(2,1)S(1)}, u32[]{:S(2)}, u32[]{:S(2)}) async-start(bf16[8,2,128]{2,1,0:T(2,128)(2,1)} %reshape.223), calls=%async_computation.1 | async-start | bytes 8192 | tf_op jit(solution)/shard_map/all_to_all | solution.py:93
  43.3 0.1 reshape.226
  43.4 0.1 fusion.63
  43.5 5.3 %all-to-all-done.1 = bf16[8,2,128]{2,1,0:T(2,128)(2,1)S(1)} async-done(((bf16[8,2,128]{2,1,0:T(2,128)(2,1)}), bf16[8,2,128]{2,1,0:T(2,128)(2,1)S(1)}, u32[]{:S(2)}, u32[]{:S(2)}) %all-to-all-start.1) | async-done | bytes 4128 | tf_op jit(solution)/shard_map/all_to_all | solution.py:93
  48.8 3.3 %all-to-all-start = ((bf16[32,2,512]{2,1,0:T(2,128)(2,1)}), bf16[32,2,512]{2,1,0:T(2,128)(2,1)S(1)}, u32[]{:S(2)}, u32[]{:S(2)}) async-start(bf16[32,2,512]{2,1,0:T(2,128)(2,1)} %copy.64), calls=%async_computation | async-start | bytes 131072 | tf_op jit(solution)/shard_map/all_to_all | solution.py:92
  52.1 0.1 reshape.224
  52.3 0.1 fusion.55
  52.5 0.2 fusion.83
  52.7 5.3 %all-to-all-done = bf16[32,2,512]{2,1,0:T(2,128)(2,1)S(1)} async-done(((bf16[32,2,512]{2,1,0:T(2,128)(2,1)}), bf16[32,2,512]{2,1,0:T(2,128)(2,1)S(1)}, u32[]{:S(2)}, u32[]{:S(2)}) %all-to-all-start) | async-done | bytes 65568 | tf_op jit(solution)/shard_map/all_to_all | solution.py:92
  58.1 3.5 %fusion.100 = f32[4,16,1024]{2,1,0:T(8,128)S(1)} fusion(bf16[4,16,512]{2,1,0:T(8,128)(2,1)S(1)} %all_to_all.58, bf16[4,1024,512]{2,1,0:T(8,128)(2,1)} %param.28), kind=kOutput, calls=%fused_computation.141 | convolution fusion | flops 67108864 | bytes 4521984 | tf_op jit(solution)/shard_map/bhr,blr->bhl/dot_general | solution.py:100
  61.6 0.1 fusion.79
  61.8 0.3 fusion.99
  62.1 0.2 fusion.37
  62.4 0.7 fusion.11
  63.1 0.7 copy.68
  63.8 3.3 %all-to-all-start.3 = ((bf16[4,16,512]{2,0,1:T(4,128)(2,1)}), bf16[4,16,512]{2,0,1:T(4,128)(2,1)S(1)}, u32[]{:S(2)}, u32[]{:S(2)}) async-start(bf16[4,16,512]{2,0,1:T(4,128)(2,1)} %copy.68), calls=%async_computation.3 | async-start | bytes 131072 | tf_op jit(solution)/shard_map/all_to_all | solution.py:132
  67.2 5.8 %all-to-all-done.3 = bf16[4,16,512]{2,0,1:T(4,128)(2,1)S(1)} async-done(((bf16[4,16,512]{2,0,1:T(4,128)(2,1)}), bf16[4,16,512]{2,0,1:T(4,128)(2,1)S(1)}, u32[]{:S(2)}, u32[]{:S(2)}) %all-to-all-start.3) | async-done | bytes 65568 | tf_op jit(solution)/shard_map/all_to_all | solution.py:132
  73.1 1.3 convolution_bitcast_fusion
  74.4 0.7 convert_element_type.163
  75.2 0.1 copy.71
  75.3 0.1 eq.39
  75.4 0.1 fusion.53
  75.5 0.2 reduce_window_sum.11
  75.7 0.2 select_reduce_fusion.1
  75.8 0.1 reduce_sum.73
  76.1 0.6 dynamic-slice.1
  77.3 0.1 fusion.52
  77.4 0.1 select_reduce_fusion
  77.5 18.5 %all-gather.4.cloned.1.call-done = bf16[256,2048]{1,0:T(8,128)(2,1)} async-done(((bf16[32,2048]{1,0:T(8,128)(2,1)}), bf16[256,2048]{1,0:T(8,128)(2,1)}) %all-gather.4.cloned.1.call-update) | async-done | bytes 1048592 | tf_op jit(solution)/shard_map/all_gather | solution.py:146
  96.0 1.4 reduce_sum.71
  97.4 0.1 multiply_reduce_fusion
  97.6 0.3 fusion.96
  97.8 0.9 fusion.2
  98.7 3.7 %all-to-all-start.4 = ((bf16[4,1,8,2048]{3,2,1,0:T(8,128)(2,1)}), bf16[4,1,8,2048]{3,2,1,0:T(8,128)(2,1)S(1)}, u32[]{:S(2)}, u32[]{:S(2)}) async-start(bf16[4,1,8,2048]{3,2,1,0:T(8,128)(2,1)} %fusion.2), calls=%async_computation.4 | async-start | bytes 262144 | tf_op jit(solution)/shard_map/all_to_all | solution.py:182
  102.4 0.3 fusion.97
  102.6 4.8 %all-to-all-done.4 = bf16[4,1,8,2048]{3,2,1,0:T(8,128)(2,1)S(1)} async-done(((bf16[4,1,8,2048]{3,2,1,0:T(8,128)(2,1)}), bf16[4,1,8,2048]{3,2,1,0:T(8,128)(2,1)S(1)}, u32[]{:S(2)}, u32[]{:S(2)}) %all-to-all-start.4) | async-done | bytes 131104 | tf_op jit(solution)/shard_map/all_to_all | solution.py:182
  107.4 2.0 %fusion.13 = f32[4,1,8,512]{3,2,0,1:T(8,128)S(1)} fusion(bf16[1,2048,512]{2,1,0:T(8,128)(2,1)} %param.42, bf16[4,1,8,2048]{3,2,1,0:T(8,128)(2,1)S(1)} %all-to-all-done.4), kind=kOutput, calls=%fused_computation.21 | convolution fusion | flops 67108864 | bytes 2293760 | tf_op jit(solution)/shard_map/sxcd,xdf->sxcf/dot_general | solution.py:183
  109.4 3.1 %fusion.3 = bf16[4,1,8,2048]{3,2,1,0:T(8,128)(2,1)} fusion(bf16[1,512,2048]{2,1,0:T(8,128)(2,1)S(1)} %copy-done, bf16[1,2048,512]{2,1,0:T(8,128)(2,1)} %param.43, bf16[4,1,8,2048]{3,2,1,0:T(8,128)(2,1)S(1)} %all-to-all-done.4, f32[4,1,8,512]{3,2,0,1:T(8,128)S(1)} %fusion.13), kind=kOutput, calls=%fused_computation.8 | convolution fusion | flops 134381568 | bytes 4521984 | tf_op jit(solution)/shard_map/sxcf,xfd->sxcd/dot_general | solution.py:188
  112.6 3.5 %all-to-all-start.5 = ((bf16[4,1,8,2048]{3,2,1,0:T(8,128)(2,1)}), bf16[4,1,8,2048]{3,2,1,0:T(8,128)(2,1)S(1)}, u32[]{:S(2)}, u32[]{:S(2)}) async-start(bf16[4,1,8,2048]{3,2,1,0:T(8,128)(2,1)} %fusion.3), calls=%async_computation.5 | async-start | bytes 262144 | tf_op jit(solution)/shard_map/all_to_all | solution.py:191
  116.1 0.2 fusion.34
  116.3 4.7 %all-to-all-done.5 = bf16[4,1,8,2048]{3,2,1,0:T(8,128)(2,1)S(1)} async-done(((bf16[4,1,8,2048]{3,2,1,0:T(8,128)(2,1)}), bf16[4,1,8,2048]{3,2,1,0:T(8,128)(2,1)S(1)}, u32[]{:S(2)}, u32[]{:S(2)}) %all-to-all-start.5) | async-done | bytes 131104 | tf_op jit(solution)/shard_map/all_to_all | solution.py:191
  121.0 0.2 fusion.38
  121.3 1.5 convolution_add_fusion
  122.8 2.2 %fusion.1 = bf16[32,2048]{1,0:T(8,128)(2,1)} fusion(f32[32,2048]{1,0:T(8,128)S(1)} %convolution_add_fusion, bf16[128,2048]{1,0:T(8,128)(2,1)S(1)} %copy-done.4, bf16[2048,128]{1,0:T(8,128)(2,1)} %param.49, f32[32]{0:T(128)S(1)} %fusion.34, f32[32,128]{1,0:T(8,128)S(1)} %fusion.96, f32[2048]{0:T(1024)S(1)} %copy-done.7, f32[32]{0:T(128)S(1)} %add_rsqrt_fusion, ...), kind=kOutput, calls=%fused_computation.4 | convolution fusion | flops 34037760 | bytes 1597696 | tf_op jit(solution)/shard_map/dot_general | solution.py:154
  125.0 0.6 pad_maximum_fusion.3
  125.6 52.6 %all-reduce.3.cloned.1.call-done = bf16[32,2048]{1,0:T(8,128)(2,1)} async-done(((bf16[32,2048]{1,0:T(8,128)(2,1)}), bf16[32,2048]{1,0:T(8,128)(2,1)}) %all-reduce.3.cloned.1.call-update) | async-done | bytes 131088
  178.2 1.4 add_convert_fusion
  (59 shorter events, 0.9 us)
Async XLA Ops:
  7.2 102.3 %copy-start = (bf16[1,512,2048]{2,1,0:T(8,128)(2,1)S(1)}, bf16[1,512,2048]{2,1,0:T(8,128)(2,1)}, u32[]{:S(2)}) copy-start(bf16[1,512,2048]{2,1,0:T(8,128)(2,1)} %param.44) | copy-start | bytes 6291460
  7.2 29.2 %copy-start.9 = (bf16[512,2,64]{0,2,1:T(8,128)(2,1)S(1)}, bf16[512,2,64]{0,2,1:T(8,128)(2,1)}, u32[]{:S(2)}) copy-start(bf16[512,2,64]{0,2,1:T(8,128)(2,1)} %param.38) | copy-start | bytes 393220
  7.2 45.2 %copy-start.12 = (f32[512]{0:T(512)S(1)}, f32[512]{0:T(512)}, u32[]{:S(2)}) copy-start(f32[512]{0:T(512)} %param.37) | copy-start | bytes 6148
  26.6 11.5 %all-to-all-start.2 = ((bf16[8,2,128]{2,1,0:T(2,128)(2,1)}), bf16[8,2,128]{2,1,0:T(2,128)(2,1)S(1)}, u32[]{:S(2)}, u32[]{:S(2)}) async-start(bf16[8,2,128]{2,1,0:T(2,128)(2,1)} %reshape.225), calls=%async_computation.2 | async-start | bytes 8192 | tf_op jit(solution)/shard_map/all_to_all | solution.py:94
  38.2 10.6 %all-to-all-start.1 = ((bf16[8,2,128]{2,1,0:T(2,128)(2,1)}), bf16[8,2,128]{2,1,0:T(2,128)(2,1)S(1)}, u32[]{:S(2)}, u32[]{:S(2)}) async-start(bf16[8,2,128]{2,1,0:T(2,128)(2,1)} %reshape.223), calls=%async_computation.1 | async-start | bytes 8192 | tf_op jit(solution)/shard_map/all_to_all | solution.py:93
  48.8 9.2 %all-to-all-start = ((bf16[32,2,512]{2,1,0:T(2,128)(2,1)}), bf16[32,2,512]{2,1,0:T(2,128)(2,1)S(1)}, u32[]{:S(2)}, u32[]{:S(2)}) async-start(bf16[32,2,512]{2,1,0:T(2,128)(2,1)} %copy.64), calls=%async_computation | async-start | bytes 131072 | tf_op jit(solution)/shard_map/all_to_all | solution.py:92
  52.5 9.1 %copy-start.11 = (bf16[4,512]{1,0:T(4,128)(2,1)}, bf16[4,512]{1,0:T(4,128)(2,1)S(1)}, u32[]{:S(2)}) copy-start(bf16[4,512]{1,0:T(4,128)(2,1)S(1)} %get-tuple-element.4) | copy-start | bytes 12292
  58.1 3.7 %copy-start.5 = (bf16[4,1024,32]{1,2,0:T(8,128)(2,1)S(1)}, bf16[4,1024,32]{1,2,0:T(8,128)(2,1)}, u32[]{:S(2)}) copy-start(bf16[4,1024,32]{1,2,0:T(8,128)(2,1)} %param.29) | copy-start | bytes 786436
  58.1 4.2 %copy-start.1 = (bf16[4,1024,512]{2,1,0:T(8,128)(2,1)S(1)}, bf16[4,1024,512]{2,1,0:T(8,128)(2,1)}, u32[]{:S(2)}) copy-start(bf16[4,1024,512]{2,1,0:T(8,128)(2,1)} %param.28) | copy-start | bytes 12582916
  62.3 10.7 %copy-start.3 = (bf16[2,64,2048]{2,1,0:T(8,128)(2,1)S(1)}, bf16[2,64,2048]{2,1,0:T(8,128)(2,1)}, u32[]{:S(2)}) copy-start(bf16[2,64,2048]{2,1,0:T(8,128)(2,1)} %param.40) | copy-start | bytes 1572868
  62.4 12.0 %copy-start.8 = (bf16[4,2048]{1,0:T(4,128)(2,1)S(1)}, bf16[4,2048]{1,0:T(4,128)(2,1)}, u32[]{:S(2)}) copy-start(bf16[4,2048]{1,0:T(4,128)(2,1)} %param.26) | copy-start | bytes 49156
  62.4 12.8 %copy-start.10 = (bf16[2048]{0:T(1024)(128)(2,1)S(1)}, bf16[2048]{0:T(1024)(128)(2,1)}, u32[]{:S(2)}) copy-start(bf16[2048]{0:T(1024)(128)(2,1)} %param.51) | copy-start | bytes 12292
  62.4 12.8 %copy-start.13 = (s32[32,4]{0,1:T(4,128)S(1)}, s32[32,4]{0,1:T(4,128)}, u32[]{:S(2)}) copy-start(s32[32,4]{0,1:T(4,128)} %param.30) | copy-start | bytes 1540
  63.1 13.0 %copy-start.15 = (u32[32]{0:T(128)S(1)}, u32[32]{0:T(128)}, u32[]{:S(2)}) copy-start(u32[32]{0:T(128)} %constant.111) | copy-start | bytes 388
  63.1 14.3 %copy-start.14 = (f32[32,4]{0,1:T(4,128)S(1)}, f32[32,4]{0,1:T(4,128)}, u32[]{:S(2)}) copy-start(f32[32,4]{0,1:T(4,128)} %param.31) | copy-start | bytes 1540
  63.1 34.4 %copy-start.2 = (bf16[2048,128]{1,0:T(8,128)(2,1)S(1)}, bf16[2048,128]{1,0:T(8,128)(2,1)}, u32[]{:S(2)}) copy-start(bf16[2048,128]{1,0:T(8,128)(2,1)} %param.48) | copy-start | bytes 1572868
  63.1 34.4 %copy-start.7 = (f32[2048]{0:T(1024)S(1)}, f32[2048]{0:T(1024)}, u32[]{:S(2)}) copy-start(f32[2048]{0:T(1024)} %param.41) | copy-start | bytes 24580
  63.8 9.2 %all-to-all-start.3 = ((bf16[4,16,512]{2,0,1:T(4,128)(2,1)}), bf16[4,16,512]{2,0,1:T(4,128)(2,1)S(1)}, u32[]{:S(2)}, u32[]{:S(2)}) async-start(bf16[4,16,512]{2,0,1:T(4,128)(2,1)} %copy.68), calls=%async_computation.3 | async-start | bytes 131072 | tf_op jit(solution)/shard_map/all_to_all | solution.py:132
  67.2 28.8 %all-gather.4.cloned.1.call-start = ((), (), s32[]{:S(2)}) async-start(), calls=%async_computation.6 | async-start | bytes 1179648 | tf_op jit(solution)/shard_map/all_gather | solution.py:146
  74.4 28.0 %copy-start.6 = (bf16[2048,64]{0,1:T(8,128)(2,1)S(1)}, bf16[2048,64]{0,1:T(8,128)(2,1)}, u32[]{:S(2)}) copy-start(bf16[2048,64]{0,1:T(8,128)(2,1)} %param.45) | copy-start | bytes 786436
  98.7 8.7 %all-to-all-start.4 = ((bf16[4,1,8,2048]{3,2,1,0:T(8,128)(2,1)}), bf16[4,1,8,2048]{3,2,1,0:T(8,128)(2,1)S(1)}, u32[]{:S(2)}, u32[]{:S(2)}) async-start(bf16[4,1,8,2048]{3,2,1,0:T(8,128)(2,1)} %fusion.2), calls=%async_computation.4 | async-start | bytes 262144 | tf_op jit(solution)/shard_map/all_to_all | solution.py:182
  112.6 10.2 %copy-start.4 = (bf16[128,2048]{1,0:T(8,128)(2,1)S(1)}, bf16[128,2048]{1,0:T(8,128)(2,1)}, u32[]{:S(2)}) copy-start(bf16[128,2048]{1,0:T(8,128)(2,1)} %param.50) | copy-start | bytes 1572868
  112.6 8.4 %all-to-all-start.5 = ((bf16[4,1,8,2048]{3,2,1,0:T(8,128)(2,1)}), bf16[4,1,8,2048]{3,2,1,0:T(8,128)(2,1)S(1)}, u32[]{:S(2)}, u32[]{:S(2)}) async-start(bf16[4,1,8,2048]{3,2,1,0:T(8,128)(2,1)} %fusion.3), calls=%async_computation.5 | async-start | bytes 262144 | tf_op jit(solution)/shard_map/all_to_all | solution.py:191
  116.0 62.2 %all-reduce.3.cloned.1.call-start = ((), (), s32[]{:S(2)}) async-start(), calls=%async_computation.7 | async-start | bytes 262144
Sparse Core Ops, SparseCore 0:
  75.3 20.7 all-gather.3
  125.1 53.1 all-reduce.2
